TPU v7x, 32 devices: a whole 2x2x4 slice. The times are simulated.
32 devices in a mesh: fs: 4 (over z), rep: 4 (over y, x), tp: 2 (over core).
Axes of the slice: x: 2, y: 2, z: 4, core: 2. Of those that a mesh axis runs over, the one named last changes fastest.
Arguments:
- normed_in: bfloat16 [16384, 2048], P(('fs', 'rep')), may hold values from -6 to 6
- inner_cot: bfloat16 [16384, 4096], P(('fs', 'rep'), 'tp'), may hold values from -6 to 6
- gated_mid: bfloat16 [16384, 4096], P(('fs', 'rep')), may hold values from -6 to 6
- output_cot: bfloat16 [16384, 2048], P(('fs', 'rep'), 'tp'), may hold values from -6 to 6
- basis_in: bfloat16 [2048, 256], replicated, may hold values from -0.125 to 0.125
- basis_mid: bfloat16 [4096, 256], replicated, may hold values from -0.09375 to 0.09375
- master_in: float32 [2048, 4096], P(('fs', 'rep'), 'tp'), may hold values from -6 to 6
- master_mid: float32 [4096, 2048], P(('fs', 'rep'), 'tp'), may hold values from -6 to 6
- first_in: float32 [256, 4096], P(('fs', 'rep'), 'tp'), may hold values from -160 to 160
- second_in: float32 [256, 4096], P(('fs', 'rep'), 'tp'), may hold values from 163.84 to 29491.2, as said below
- first_mid: float32 [256, 2048], P(('fs', 'rep'), 'tp'), may hold values from -160 to 160
- second_mid: float32 [256, 2048], P(('fs', 'rep'), 'tp'), may hold values from 163.84 to 29491.2, as said below
Outputs:
- step_in: float32 [2048, 4096], P(('fs', 'rep'), 'tp')
- step_mid: float32 [4096, 2048], P(('fs', 'rep'), 'tp')
- moment_in: float32 [256, 4096], P(('fs', 'rep'), 'tp')
- square_in: float32 [256, 4096], P(('fs', 'rep'), 'tp')
- moment_mid: float32 [256, 2048], P(('fs', 'rep'), 'tp')
- square_mid: float32 [256, 2048], P(('fs', 'rep'), 'tp')
- copy_in: bfloat16 [2048, 4096], P('fs', 'tp')
- copy_mid: bfloat16 [4096, 2048], P('fs', 'tp')
Inputs may be any that keep to these rules, and one draw needn't show every extreme that they name: `second_in`: positive second moments. `second_mid`: positive second moments.
All inputs are finite; a program needn't handle non-finite values.
Results may differ from a plain program's by a relative error of at most 0.0036.
Values may be sent and summed in bfloat16 or wider, within the bound.
A program may use at most 128 MiB of HBM per device.

v0:
```python
import jax
import jax.numpy as jnp
from jax import lax
from jax.sharding import PartitionSpec as P

D = 2048
DI = 4096
RANK = 256


beta_one = 0.9
beta_two = 0.95
rate_scale = 0.5


def contract_rows(left, right):
    return lax.dot_general(
        left, right, (((0,), (0,)), ((), ())), preferred_element_type=jnp.float32
    )


def moments(first, second, proj):
    moment = beta_one * first + (1.0 - beta_one) * proj
    square = beta_two * second + (1.0 - beta_two) * proj * proj
    return (moment, square, moment / jnp.sqrt(square))


def body(
    normed_in,
    inner_cot,
    gated_mid,
    output_cot,
    basis_in,
    basis_mid,
    master_in,
    master_mid,
    first_in,
    second_in,
    first_mid,
    second_mid,
):
    slot = lax.axis_index(("fs", "rep"))
    rows_in = master_in.shape[0]
    rows_mid = master_mid.shape[0]
    cols_in = master_in.shape[1]
    own_in = lax.dynamic_slice_in_dim(basis_in, slot * rows_in, rows_in, 0).astype(jnp.float32)
    own_mid = lax.dynamic_slice_in_dim(basis_mid, slot * rows_mid, rows_mid, 0).astype(jnp.float32)
    low_in = jnp.dot(normed_in, basis_in, preferred_element_type=jnp.float32)
    low_mid = jnp.dot(gated_mid, basis_mid, preferred_element_type=jnp.float32)
    high_in = low_in.astype(jnp.bfloat16)
    rest_in = (low_in - high_in.astype(jnp.float32)).astype(jnp.bfloat16)
    high_mid = low_mid.astype(jnp.bfloat16)
    rest_mid = (low_mid - high_mid.astype(jnp.float32)).astype(jnp.bfloat16)
    upper_in = contract_rows(high_in, inner_cot)
    lower_in = contract_rows(rest_in, inner_cot)
    upper_mid = contract_rows(high_mid, output_cot)
    lower_mid = contract_rows(rest_mid, output_cot)
    joined = lax.psum_scatter(
        jnp.concatenate([upper_in + lower_in, upper_mid + lower_mid], axis=1),
        ("fs", "rep"),
        scatter_dimension=0,
        tiled=True,
    )
    proj_in = joined[:, :cols_in]
    proj_mid = joined[:, cols_in:]
    moment_in, square_in, course_in = moments(first_in, second_in, proj_in)
    moment_mid, square_mid, course_mid = moments(first_mid, second_mid, proj_mid)
    total_in, total_mid = lax.psum(
        (jnp.sum(course_in * course_in), jnp.sum(course_mid * course_mid)), ("fs", "rep", "tp")
    )
    scale_in = rate_scale * lax.rsqrt(total_in / (RANK * DI) + 1e-06)
    scale_mid = rate_scale * lax.rsqrt(total_mid / (RANK * D) + 1e-06)
    update_in = jnp.dot(
        own_in,
        lax.all_gather(course_in, ("fs", "rep"), axis=0, tiled=True),
        precision=lax.Precision.HIGHEST,
    )
    update_mid = jnp.dot(
        own_mid,
        lax.all_gather(course_mid, ("fs", "rep"), axis=0, tiled=True),
        precision=lax.Precision.HIGHEST,
    )
    step_in = scale_in * update_in
    step_mid = scale_mid * update_mid
    fresh_in = (master_in - step_in).astype(jnp.bfloat16)
    fresh_mid = (master_mid - step_mid).astype(jnp.bfloat16)
    copy_in, copy_mid = (
        lax.all_gather(fresh_in, "rep", axis=0, tiled=True),
        lax.all_gather(fresh_mid, "rep", axis=0, tiled=True),
    )
    return (step_in, step_mid, moment_in, square_in, moment_mid, square_mid, copy_in, copy_mid)


def solution(mesh):
    in_specs = (
        P(("fs", "rep"), None),
        P(("fs", "rep"), "tp"),
        P(("fs", "rep"), None),
        P(("fs", "rep"), "tp"),
        P(),
        P(),
        P(("fs", "rep"), "tp"),
        P(("fs", "rep"), "tp"),
        P(("fs", "rep"), "tp"),
        P(("fs", "rep"), "tp"),
        P(("fs", "rep"), "tp"),
        P(("fs", "rep"), "tp"),
    )
    out_specs = (
        P(("fs", "rep"), "tp"),
        P(("fs", "rep"), "tp"),
        P(("fs", "rep"), "tp"),
        P(("fs", "rep"), "tp"),
        P(("fs", "rep"), "tp"),
        P(("fs", "rep"), "tp"),
        P("fs", "tp"),
        P("fs", "tp"),
    )
    return jax.shard_map(body, mesh=mesh, in_specs=in_specs, out_specs=out_specs, check_vma=False)
```

profile of v0, /device:TPU:0, one launch (start us, length us, event | category | flops | bytes accessed | tf_op | source)
XLA Modules:
  0.0 364.7 jit_solution(3421644763818969438)
XLA Ops:
  7.2 0.0 copy-start
  7.2 0.0 reduce-scatter.2.cloned.1.call-start
  7.2 1.5 copy-done
  8.8 0.0 copy-start.2
  8.8 5.9 %fusion.15 = f32[1024,256]{1,0:T(8,128)S(1)} fusion(bf16[1024,4096]{1,0:T(8,128)(2,1)} %param.14, bf16[4096,256]{1,0:T(8,128)(2,1)S(1)} %copy-done), kind=kOutput, calls=%fused_computation.30 | convolution fusion | flops 2147483648 | bytes 11534336 | tf_op jit(solution)/shard_map/dot_general | solution.py:49
  14.6 0.0 copy-done.2
  14.6 0.7 fusion.1
  15.4 0.0 copy-start.9
  15.4 0.0 copy-start.10
  15.4 0.7 convolution_add_fusion.1
  16.1 0.5 copy-done.9
  16.6 1.3 copy-done.10
  17.9 0.0 copy-start.1
  17.9 1.2 fusion.14
  19.2 0.9 copy-done.1
  20.1 1.3 fusion.4
  21.4 1.3 convolution_add_fusion
  22.6 1.9 pad_maximum_fusion
  24.5 0.0 copy-start.7
  24.5 0.0 copy-start.8
  24.5 0.0 copy-start.5
  24.5 0.0 copy-start.6
  24.5 0.0 copy-start.4
  24.5 0.0 reduce-scatter.2.cloned.1.call-update
  24.6 0.0 all-gather.7.cloned.1.call-start
  24.6 135.1 %reduce-scatter.2.cloned.1.call-done = f32[16,3072]{1,0:T(8,128)} async-done(((f32[256,3072]{1,0:T(8,128)}), f32[16,3072]{1,0:T(8,128)}) %reduce-scatter.2.cloned.1.call-update) | async-done | bytes 196624 | tf_op jit(solution)/shard_map/reduce_scatter | solution.py:58
  159.7 0.0 copy-done.7
  159.7 0.0 copy-done.8
  159.7 2.1 multiply_reduce_fusion.1
  161.8 0.0 all-gather.7.cloned.1.call-update
  161.8 0.0 all-gather.5.cloned.1.call-start
  161.9 0.0 copy-done.5
  161.9 0.0 copy-done.6
  161.9 2.3 multiply_reduce_fusion
  164.1 0.0 all-gather.5.cloned.1.call-update
  164.2 0.0 all-gather.11.cloned.1.call-start
  164.2 40.2 %all-reduce = (f32[]{:T(128)}, f32[]{:T(128)}) all-reduce(f32[]{:T(128)} %get-tuple-element.14, f32[]{:T(128)} %get-tuple-element.10), channel_id=1, replica_groups=mesh['fs'=4,'rep'=4,'tp'=2] {'fs','rep','tp'}, use_global_device_ids=true, to_apply=%region_2.0 | all-reduce | flops 2 | bytes 16 | tf_op jit(solution)/shard_map/psum | solution.py:68
  205.1 12.0 %all-gather.7.cloned.1.call-done = f32[256,1024]{1,0:T(8,128)} async-done(((f32[16,1024]{1,0:T(8,128)}), f32[256,1024]{1,0:T(8,128)}) %all-gather.7.cloned.1.call-update) | async-done | bytes 1048592 | tf_op jit(solution)/shard_map/all_gather | solution.py:80
  217.2 0.0 copy-done.4
  217.2 3.1 subtract_convert_fusion
  220.2 0.0 all-gather.11.cloned.1.call-update
  220.2 0.0 all-gather.9.cloned.1.call-start
  221.0 58.8 %all-gather.5.cloned.1.call-done = f32[256,2048]{1,0:T(8,128)} async-done(((f32[16,2048]{1,0:T(8,128)}), f32[256,2048]{1,0:T(8,128)}) %all-gather.5.cloned.1.call-update) | async-done | bytes 2097168 | tf_op jit(solution)/shard_map/all_gather | solution.py:75
  279.8 3.9 %subtract_convert_fusion.1 = (bf16[128,2048]{1,0:T(8,128)(2,1)}, f32[128,2048]{1,0:T(8,128)}) fusion(f32[128,2048]{1,0:T(8,128)} %param.18, f32[256,2048]{1,0:T(8,128)} %all-gather.5.cloned.1.call-done, bf16[2048,256]{1,0:T(8,128)(2,1)} %param.16, s32[]{:T(128)S(6)} %select_n.6, f32[]{:T(128)S(6)} %mul.97), kind=kOutput, calls=%fused_computation.6 | convolution fusion | flops 806092800 | bytes 4784136 | tf_op jit(solution)/shard_map/dot_general | solution.py:73
  283.7 0.0 all-gather.9.cloned.1.call-update
  283.7 32.3 %all-gather.11.cloned.1.call-done = bf16[1024,1024]{1,0:T(8,128)(2,1)} async-done(((bf16[256,1024]{1,0:T(8,128)(2,1)}), bf16[1024,1024]{1,0:T(8,128)(2,1)}) %all-gather.11.cloned.1.call-update) | async-done | bytes 2097168 | tf_op jit(solution)/shard_map/all_gather | solution.py:89
  316.0 37.5 %all-gather.9.cloned.1.call-done = bf16[512,2048]{1,0:T(8,128)(2,1)} async-done(((bf16[128,2048]{1,0:T(8,128)(2,1)}), bf16[512,2048]{1,0:T(8,128)(2,1)}) %all-gather.9.cloned.1.call-update) | async-done | bytes 2097168 | tf_op jit(solution)/shard_map/all_gather | solution.py:88
  353.5 0.0 copy-start.3
  353.5 3.3 copy.22
  356.8 0.0 copy-done.3
  356.8 1.3 copy.23
Async XLA Ops:
  7.2 1.6 copy-start
  7.2 152.5 %reduce-scatter.2.cloned.1.call-start = ((), (), s32[]{:S(2)}) async-start(), calls=%async_computation.1 | async-start | bytes 3342336 | tf_op jit(solution)/shard_map/reduce_scatter | solution.py:58
  8.8 5.9 %copy-start.2 = (bf16[1024,1024]{1,0:T(8,128)(2,1)S(1)}, bf16[1024,1024]{1,0:T(8,128)(2,1)}, u32[]{:S(2)}) copy-start(bf16[1024,1024]{1,0:T(8,128)(2,1)} %param.15) | copy-start | bytes 6291460
  15.4 1.2 copy-start.9
  15.4 2.5 copy-start.10
  17.9 2.2 copy-start.1
  24.5 135.2 %copy-start.7 = (f32[16,1024]{1,0:T(8,128)S(1)}, f32[16,1024]{1,0:T(8,128)}, u32[]{:S(2)}) copy-start(f32[16,1024]{1,0:T(8,128)} %param.23) | copy-start | bytes 196612
  24.5 135.2 %copy-start.8 = (f32[16,1024]{1,0:T(8,128)S(1)}, f32[16,1024]{1,0:T(8,128)}, u32[]{:S(2)}) copy-start(f32[16,1024]{1,0:T(8,128)} %param.22) | copy-start | bytes 196612
  24.5 137.3 %copy-start.5 = (f32[16,2048]{1,0:T(8,128)S(1)}, f32[16,2048]{1,0:T(8,128)}, u32[]{:S(2)}) copy-start(f32[16,2048]{1,0:T(8,128)} %param.21) | copy-start | bytes 393220
  24.5 137.4 %copy-start.6 = (f32[16,2048]{1,0:T(8,128)S(1)}, f32[16,2048]{1,0:T(8,128)}, u32[]{:S(2)}) copy-start(f32[16,2048]{1,0:T(8,128)} %param.20) | copy-start | bytes 393220
  24.5 192.6 %copy-start.4 = (f32[256,1024]{1,0:T(8,128)S(1)}, f32[256,1024]{1,0:T(8,128)}, u32[]{:S(2)}) copy-start(f32[256,1024]{1,0:T(8,128)} %param.19) | copy-start | bytes 3145732
  24.6 192.6 %all-gather.7.cloned.1.call-start = ((), (), s32[]{:S(2)}) async-start(), calls=%async_computation.3 | async-start | bytes 1114112 | tf_op jit(solution)/shard_map/all_gather | solution.py:80
  161.8 118.0 %all-gather.5.cloned.1.call-start = ((), (), s32[]{:S(2)}) async-start(), calls=%async_computation.2 | async-start | bytes 2228224 | tf_op jit(solution)/shard_map/all_gather | solution.py:75
  164.2 151.9 %all-gather.11.cloned.1.call-start = ((), (), s32[]{:S(2)}) async-start(), calls=%async_computation.5 | async-start | bytes 2621440 | tf_op jit(solution)/shard_map/all_gather | solution.py:89
  220.2 133.3 %all-gather.9.cloned.1.call-start = ((), (), s32[]{:S(2)}) async-start(), calls=%async_computation.4 | async-start | bytes 2621440 | tf_op jit(solution)/shard_map/all_gather | solution.py:88
  353.5 3.3 copy-start.3
Sparse Core Ops, SparseCore 0:
  24.7 134.9 reduce-scatter.1
  163.0 54.1 all-gather.6
  220.5 59.2 all-gather.4
  282.0 33.9 all-gather.10
  318.3 35.1 all-gather.8
where the time goes:
time: 365 us
  waiting for transfers between devices  276 us (76%)
  blocking collectives  40.2 us (11%)
  matrix products  18.1 us (5%)
  between operations  15.3 us (4%)
  local copies, waits for them, and re-layouts  8.9 us (2%)
  other arithmetic  6.25 us (2%)
    reduce_scatter x1, waiting for transfers between devices, body(): lax.psum_scatter(jnp.concatenate([upper_in + lower_in, upper_mid + lower_...  135 us
    all_gather x1, waiting for transfers between devices, body(): lax.all_gather(course_in, ('fs', 'rep'), axis=0, tiled=True)  58.8 us
    psum x1, blocking collectives, body(): lax.psum((jnp.sum(course_in * course_in), jnp.sum(course_mid * course_mid...  40.2 us
    all_gather x1, waiting for transfers between devices, body(): lax.all_gather(fresh_in, 'rep', axis=0, tiled=True)  37.5 us
    all_gather x1, waiting for transfers between devices, body(): lax.all_gather(fresh_mid, 'rep', axis=0, tiled=True)  32.3 us
    all_gather x1, waiting for transfers between devices, body(): lax.all_gather(course_mid, ('fs', 'rep'), axis=0, tiled=True)  12 us
    unnamed x24, local copies, waits for them, and re-layouts  8.9 us
  transfers between devices with their start and end apart: 5, of which 5 were waited for; matrix products, arithmetic and copies ran while one was open for 3% of the time, Pallas kernels for 0%

commit v1 on v0

v1 whole, which is shorter than its diff:
```python
import functools

import jax
import jax.numpy as jnp
from jax import lax
from jax.experimental import pallas as pl
from jax.experimental.pallas import tpu as pltpu
from jax.sharding import PartitionSpec as P

beta_one = 0.9
beta_two = 0.95
rate_scale = 0.5

MESH = pl.DeviceIdType.MESH


def remote(src, dst, send, recv, where):
    return pltpu.make_async_remote_copy(
        src_ref=src, dst_ref=dst, send_sem=send, recv_sem=recv, device_id=where, device_id_type=MESH
    )


def exchange(
    sizes,
    low_in, low_mid, cot_in, cot_mid, master_in, master_mid,
    first_in, second_in, first_mid, second_mid,
    ways, weights_in, weights_mid, moment_in, square_in, moment_mid, square_mid, totals,
    cots, whole, own, part, zland, spread, xland, sums,
    cot_sem, zsend, zrecv, xsend, xrecv, msend, mrecv, mlocal, gzs, gxs, gys, gdiag, grecv, tsend, trecv,
):
    F, R, T, rows, width, n_in, n_mid = sizes
    nt = n_in + n_mid
    rank = F * R * rows
    f, r, t = lax.axis_index("fs"), lax.axis_index("rep"), lax.axis_index("tp")
    cols_in = n_in * width

    def cot_copy(c, source, base):
        return pltpu.make_async_copy(
            source.at[:, pl.ds(pl.multiple_of((c - base) * width, width), width)], cots.at[c], cot_sem.at[c]
        )

    for c in range(nt):
        (cot_copy(c, cot_in, 0) if c < n_in else cot_copy(c, cot_mid, n_in)).start()
    local_in = pltpu.make_async_copy(master_in, weights_in.at[r], mlocal.at[0])
    local_mid = pltpu.make_async_copy(master_mid, weights_mid.at[r], mlocal.at[1])
    local_in.start()
    local_mid.start()

    barrier = pltpu.get_barrier_semaphore()
    for k in range(1, F):
        pl.semaphore_signal(barrier, inc=1, device_id={"fs": lax.rem(f + k, F)}, device_id_type=MESH)
    for k in range(1, R):
        pl.semaphore_signal(barrier, inc=1, device_id={"rep": lax.rem(r + k, R)}, device_id_type=MESH)
    for k in range(1, T):
        pl.semaphore_signal(barrier, inc=1, device_id={"tp": lax.rem(t + k, T)}, device_id_type=MESH)
    pl.semaphore_wait(barrier, F + R + T - 3)

    half = R // 2
    high, low = r // half, lax.rem(r, half)
    near = high * half + (half - 1 - low)
    far = (1 - high) * half + low
    cross = (1 - high) * half + (half - 1 - low)

    def m_copy(which, source, peer, slot, index):
        array = weights_in if which == 0 else weights_mid
        return remote(source, array.at[slot], msend.at[index], mrecv.at[index], {"rep": peer})

    m_sends = [
        m_copy(0, master_in, near, r, 0),
        m_copy(1, master_mid, far, r, 1),
        m_copy(1, master_mid, near, r, 2),
        m_copy(0, master_in, far, r, 3),
    ]
    m_recvs = [
        m_copy(0, master_in, near, near, 0),
        m_copy(1, master_mid, far, far, 1),
        m_copy(1, master_mid, near, near, 2),
        m_copy(0, master_in, far, far, 3),
        m_copy(0, master_in, far, cross, 4),
        m_copy(1, master_mid, near, cross, 5),
    ]
    for copy in m_sends:
        copy.start()

    def z_copy(c, peer, slot, to):
        return remote(part.at[c, peer], zland.at[c, slot], zsend.at[c, peer], zrecv.at[c, slot], {"fs": to})

    def contract(low_ref, source, base, c):
        cot_copy(c, source, base).wait()
        both = jnp.dot(low_ref[...], cots[c], preferred_element_type=jnp.float32)
        joint = (both[:rank] + both[rank:]).reshape(F, R * rows, width)
        whole[...] = joint
        part[c] = joint.astype(jnp.bfloat16)
        own[c] = whole[f]
        for k in range(1, F):
            peer = lax.rem(f + k, F)
            z_copy(c, peer, f, peer).start()

    @pl.loop(0, n_in)
    def _(c):
        contract(low_in, cot_in, 0, c)

    @pl.loop(n_in, nt)
    def _(c):
        contract(low_mid, cot_mid, n_in, c)

    def x_copy(c, peer, slot):
        return remote(spread.at[c, peer], xland.at[c, slot], xsend.at[c, peer], xrecv.at[c, slot], {"rep": peer})

    def gather_sum(c):
        total = own[c]
        for k in range(1, F):
            peer = lax.rem(f + k, F)
            z_copy(c, peer, peer, peer).wait_recv()
            total = total + zland[c, peer].astype(jnp.float32)
        for k in range(R):
            spread[c, k] = total[k * rows : (k + 1) * rows]
        for k in range(1, R):
            peer = lax.rem(r + k, R)
            x_copy(c, peer, r).start()

    def update(c):
        proj = spread[c, r]
        for k in range(1, R):
            peer = lax.rem(r + k, R)
            x_copy(c, peer, peer).wait_recv()
            proj = proj + xland[c, peer]
        if c < n_in:
            span = slice(c * width, (c + 1) * width)
            first, second, moment_ref, square_ref = first_in, second_in, moment_in, square_in
        else:
            span = slice((c - n_in) * width, (c - n_in + 1) * width)
            first, second, moment_ref, square_ref = first_mid, second_mid, moment_mid, square_mid
        moment = beta_one * first[:, span] + (1.0 - beta_one) * proj
        square = beta_two * second[:, span] + (1.0 - beta_two) * proj * proj
        moment_ref[:, span] = moment
        square_ref[:, span] = square
        ways[f, r, :, c * width : (c + 1) * width] = (moment / jnp.sqrt(square)).astype(jnp.bfloat16)

    relays = [
        m_copy(0, weights_in.at[near], far, near, 4),
        m_copy(1, weights_mid.at[far], near, far, 5),
    ]
    relay_at = nt // 2
    for c in range(nt):
        gather_sum(c)
        if c == relay_at:
            m_recvs[0].wait_recv()
            relays[0].start()
            m_recvs[1].wait_recv()
            relays[1].start()
        if c > 0:
            update(c - 1)
    update(nt - 1)

    def g_copy(i, j, send, where):
        return remote(ways.at[i, j], ways.at[i, j], send, grecv.at[i, j], where)

    for k in range(1, F):
        peer = lax.rem(f + k, F)
        g_copy(f, r, gzs.at[k], {"fs": peer}).start()

    def onward(k):
        i = lax.rem(f + k, F)
        if k > 0:
            g_copy(i, r, gzs.at[k], {"fs": i}).wait_recv()
        g_copy(i, r, gxs.at[k], {"rep": near}).start()
        g_copy(i, r, gys.at[k], {"rep": far}).start()

    def relay(k):
        i = lax.rem(f + k, F)
        if k % 2 == 0:
            g_copy(i, near, gdiag.at[k], {"rep": far}).wait_recv()
            g_copy(i, near, gdiag.at[k], {"rep": far}).start()
        else:
            g_copy(i, far, gdiag.at[k], {"rep": near}).wait_recv()
            g_copy(i, far, gdiag.at[k], {"rep": near}).start()

    onward(0)
    for k in range(1, F):
        onward(k)
        relay(k - 1)
    relay(F - 1)
    for k in range(F):
        i = lax.rem(f + k, F)
        g_copy(i, far if k % 2 == 0 else near, gdiag.at[k], {"rep": far}).wait_recv()
        g_copy(i, cross, gdiag.at[k], {"rep": far}).wait_recv()

    square_sum = jnp.zeros((rows, nt * width), jnp.float32)

    def add_piece(i, acc):
        for j in range(R):
            piece = ways[i, j].astype(jnp.float32)
            acc = acc + piece * piece
        return acc

    square_sum = lax.fori_loop(0, F, add_piece, square_sum)
    sums[t, 0] = jnp.full(sums.shape[2:], jnp.sum(square_sum[:, :cols_in]), jnp.float32)
    sums[t, 1] = jnp.full(sums.shape[2:], jnp.sum(square_sum[:, cols_in:]), jnp.float32)

    def t_copy(peer, slot):
        return remote(sums.at[slot], sums.at[slot], tsend.at[peer], trecv.at[slot], {"tp": peer})

    for k in range(1, T):
        t_copy(lax.rem(t + k, T), t).start()

    for index in range(2, 6):
        m_recvs[index].wait_recv()
    for copy in m_sends + relays:
        copy.wait_send()
    local_in.wait()
    local_mid.wait()
    for k in range(1, F):
        peer = lax.rem(f + k, F)
        for c in range(nt):
            z_copy(c, peer, f, peer).wait_send()
        g_copy(f, r, gzs.at[k], {"fs": peer}).wait_send()
    for k in range(1, R):
        peer = lax.rem(r + k, R)
        for c in range(nt):
            x_copy(c, peer, r).wait_send()
    for k in range(F):
        i = lax.rem(f + k, F)
        g_copy(i, r, gxs.at[k], {"rep": near}).wait_send()
        g_copy(i, r, gys.at[k], {"rep": far}).wait_send()
        g_copy(i, near, gdiag.at[k], {"rep": far}).wait_send()
    for k in range(1, T):
        peer = lax.rem(t + k, T)
        t_copy(peer, peer).wait_recv()
        t_copy(peer, t).wait_send()
    total = sums[0]
    for k in range(1, T):
        total = total + sums[k]
    totals[...] = total


def body(
    shape,
    normed_in, inner_cot, gated_mid, output_cot, basis_in, basis_mid,
    master_in, master_mid, first_in, second_in, first_mid, second_mid,
):
    F, R, T = shape
    rank = basis_in.shape[1]
    rows, cols_in = first_in.shape
    cols_mid = first_mid.shape[1]
    tokens = normed_in.shape[0]
    width = 512
    n_in, n_mid = cols_in // width, cols_mid // width
    nt = n_in + n_mid

    def split(basis, inputs):
        lowered = lax.dot_general(basis, inputs, (((0,), (1,)), ((), ())), preferred_element_type=jnp.float32)
        upper = lowered.astype(jnp.bfloat16)
        lower = (lowered - upper.astype(jnp.float32)).astype(jnp.bfloat16)
        return jnp.concatenate([upper, lower], axis=0)

    low_in = split(basis_in, normed_in)
    low_mid = split(basis_mid, gated_mid)
    rough_in = master_in.astype(jnp.bfloat16)
    rough_mid = master_mid.astype(jnp.bfloat16)

    vmem = pl.BlockSpec(memory_space=pltpu.VMEM)
    anywhere = pl.BlockSpec(memory_space=pl.ANY)
    dma = pltpu.SemaphoreType.DMA
    f32, bf16 = jnp.float32, jnp.bfloat16
    small = jax.ShapeDtypeStruct
    ways, weights_in, weights_mid, moment_in, square_in, moment_mid, square_mid, totals = pl.pallas_call(
        functools.partial(exchange, (F, R, T, rows, width, n_in, n_mid)),
        out_shape=(
            small((F, R, rows, nt * width), bf16),
            small((R,) + master_in.shape, bf16),
            small((R,) + master_mid.shape, bf16),
            small(first_in.shape, f32),
            small(first_in.shape, f32),
            small(first_mid.shape, f32),
            small(first_mid.shape, f32),
            small((2, 8, 128), f32),
        ),
        in_specs=[vmem, vmem, anywhere, anywhere, vmem, vmem, vmem, vmem, vmem, vmem],
        out_specs=(vmem, anywhere, anywhere, vmem, vmem, vmem, vmem, vmem),
        scratch_shapes=[
            pltpu.VMEM((nt, tokens, width), bf16),
            pltpu.VMEM((F, R * rows, width), f32),
            pltpu.VMEM((nt, R * rows, width), f32),
            pltpu.VMEM((nt, F, R * rows, width), bf16),
            pltpu.VMEM((nt, F, R * rows, width), bf16),
            pltpu.VMEM((nt, R, rows, width), f32),
            pltpu.VMEM((nt, R, rows, width), f32),
            pltpu.VMEM((T, 2, 8, 128), f32),
            dma((nt,)),
            dma((nt, F)),
            dma((nt, F)),
            dma((nt, R)),
            dma((nt, R)),
            dma((6,)),
            dma((6,)),
            dma((2,)),
            dma((F,)),
            dma((F,)),
            dma((F,)),
            dma((F,)),
            dma((F, R)),
            dma((T,)),
            dma((T,)),
        ],
        compiler_params=pltpu.CompilerParams(
            collective_id=0, has_side_effects=True, vmem_limit_bytes=48 * 1024 * 1024
        ),
    )(
        low_in, low_mid, inner_cot, output_cot, rough_in, rough_mid,
        first_in, second_in, first_mid, second_mid,
    )

    f, slot = lax.axis_index("fs"), lax.axis_index(("fs", "rep"))
    flat = ways.reshape(rank, nt * width)

    def finish(total, columns, basis, master, weights, way):
        scale = rate_scale * lax.rsqrt(total / (rank * columns * T) + 1e-06)
        count = master.shape[0]
        mine = lax.dynamic_slice_in_dim(basis, slot * count, count, 0)
        group = lax.dynamic_slice_in_dim(basis, f * count * R, count * R, 0)
        step = scale * jnp.dot(mine, way, preferred_element_type=f32)
        course = scale * jnp.dot(group, way, preferred_element_type=f32)
        copy = (weights.reshape(count * R, columns).astype(f32) - course).astype(bf16)
        return step, copy

    step_in, copy_in = finish(totals[0, 0, 0], cols_in, basis_in, master_in, weights_in, flat[:, :cols_in])
    step_mid, copy_mid = finish(totals[1, 0, 0], cols_mid, basis_mid, master_mid, weights_mid, flat[:, cols_in:])
    return (step_in, step_mid, moment_in, square_in, moment_mid, square_mid, copy_in, copy_mid)


def solution(mesh):
    both = P(("fs", "rep"), "tp")
    in_specs = (
        P(("fs", "rep"), None), both, P(("fs", "rep"), None), both, P(), P(),
        both, both, both, both, both, both,
    )
    out_specs = (both, both, both, both, both, both, P("fs", "tp"), P("fs", "tp"))
    shape = (mesh.shape["fs"], mesh.shape["rep"], mesh.shape["tp"])
    return jax.shard_map(
        functools.partial(body, shape), mesh=mesh, in_specs=in_specs, out_specs=out_specs, check_vma=False
    )
```

time: 365 us -> 102 us (0.28)
  waiting for transfers between devices: 276 us -> 0 us
  Pallas kernels: 0 us -> 72.2 us
  blocking collectives: 40.2 us -> 0 us
  between operations: 15.3 us -> 2.21 us
  other arithmetic: 6.25 us -> 0.3 us
    all_gather x4 -> x0, waiting for transfers between devices: 141 us -> none  [the longest x1 58.8 us: body(): lax.all_gather(course_in, ('fs', 'rep'), axis=0, tiled=True)]
    reduce_scatter x1 -> x0, waiting for transfers between devices: 135 us -> none  [body(): lax.psum_scatter(jnp.concatenate([upper_in + lower_in, upper_mid + lower_...]
    pallas_call x0 -> x1, Pallas kernels: none -> 72.2 us  [body(): pl.pallas_call(functools.partial(exchange, (F, R, T, rows, width, n_in, n...]
    psum x1 -> x0, blocking collectives: 40.2 us -> none  [body(): lax.psum((jnp.sum(course_in * course_in), jnp.sum(course_mid * course_mid...]
    reduce_sum x2 -> x0, other arithmetic: 4.39 us -> none  [the longest x1 2.27 us: body(): jnp.sum(course_in * course_in)]
    dot_general x8 -> x6, matrix products: 18.1 us -> 20.2 us  [the longest x2 7.77 us: finish(): course = scale * jnp.dot(group, way, preferred_element_type=f32)]
  transfers between devices with their start and end apart: 5 -> 0, of which waited for: 5 -> 0; matrix products, arithmetic and copies ran while one was open for 3% -> 0% of each run, Pallas kernels for 0% -> 0%
where the time goes in v1:
time: 102 us
  Pallas kernels  72.2 us (71%)
  matrix products  20.2 us (20%)
  local copies, waits for them, and re-layouts  7.11 us (7%)
  between operations  2.21 us (2%)
    pallas_call x1, Pallas kernels, body(): pl.pallas_call(functools.partial(exchange, (F, R, T, rows, width, n_in, n...  72.2 us
    dot_general x2, matrix products, finish(): course = scale * jnp.dot(group, way, preferred_element_type=f32)  7.77 us
    dot_general x2, matrix products, split(): lax.dot_general(basis, inputs, (((0,), (1,)), ((), ())), preferred_elemen...  7.61 us
    unnamed x24, local copies, waits for them, and re-layouts  6.59 us
    dot_general x2, matrix products, finish(): step = scale * jnp.dot(mine, way, preferred_element_type=f32)  4.82 us

profile of v1, /device:TPU:0, one launch (start us, length us, event | category | flops | bytes accessed | tf_op | source)
XLA Modules:
  0.0 102.0 jit_solution(7232915944803401106)
XLA Ops:
  0.6 0.0 copy-start
  0.6 0.0 copy-start.9
  0.7 0.0 copy-start.8
  0.7 1.6 %copy-done = bf16[4096,256]{1,0:T(8,128)(2,1)S(1)} copy-done((bf16[4096,256]{1,0:T(8,128)(2,1)S(1)}, bf16[4096,256]{1,0:T(8,128)(2,1)}, u32[]{:S(2)}) %copy-start) | copy-done | bytes 2097176
  2.2 6.3 %subtract_convert_fusion = (bf16[256,1024]{1,0:T(8,128)(2,1)S(1)}, bf16[256,1024]{1,0:T(8,128)(2,1)S(1)}) fusion(bf16[4096,256]{1,0:T(8,128)(2,1)S(1)} %copy-done, bf16[1024,4096]{1,0:T(8,128)(2,1)} %param.14), kind=kOutput, calls=%fused_computation.8 | convolution fusion | flops 2148532224 | bytes 11534336 | tf_op jit(solution)/shard_map/dot_general | solution.py:252
  8.6 0.0 copy-done.9
  8.6 0.0 copy-done.8
  8.6 1.3 %subtract_convert_fusion.1 = (bf16[256,1024]{1,0:T(8,128)(2,1)S(1)}, bf16[256,1024]{1,0:T(8,128)(2,1)S(1)}) fusion(bf16[2048,256]{1,0:T(8,128)(2,1)S(1)} %copy-done.8, bf16[1024,2048]{1,0:T(8,128)(2,1)S(1)} %copy-done.9), kind=kOutput, calls=%fused_computation.9 | convolution fusion | flops 1074790400 | bytes 6291456 | tf_op jit(solution)/shard_map/dot_general | solution.py:252
  9.9 0.0 copy-start.6
  9.9 0.0 copy-start.7
  9.9 0.2 pad_maximum_fusion
  10.1 0.0 copy-start.2
  10.1 0.0 copy-start.3
  10.1 0.0 copy-start.4
  10.1 0.0 copy-start.5
  10.1 1.0 copy-done.6
  11.1 0.1 convert_element_type.48.master_in
  11.2 0.3 copy-done.7
  11.4 0.1 convert_element_type.49.master_mid
  11.5 0.0 copy-done.2
  11.5 0.0 copy-done.3
  11.5 0.0 copy-done.4
  11.5 0.0 copy-done.5
  11.5 72.2 %shard_map.179 = (bf16[4,4,16,3072]{3,2,1,0:T(8,128)(2,1)S(1)}, bf16[4,128,2048]{2,1,0:T(8,128)(2,1)}, bf16[4,256,1024]{2,1,0:T(8,128)(2,1)}, f32[16,2048]{1,0:T...) custom-call(bf16[512,1024]{1,0:T(8,128)(2,1)S(1)} %get-tuple-element, ...), custom_call_target="tpu_custom_call" | custom-call | tf_op jit(solution)/shard_map/pallas_call | solution.py:267
  83.8 0.0 copy-start.1
  83.8 1.2 %copy-done.1 = bf16[4,4,16,3072]{3,2,1,0:T(8,128)(2,1)} copy-done((bf16[4,4,16,3072]{3,2,1,0:T(8,128)(2,1)}, bf16[4,4,16,3072]{3,2,1,0:T(8,128)(2,1)S(1)}, u32[]{:S(2)}) %copy-start.1) | copy-done | bytes 1572888
  85.0 0.5 fusion.14
  86.2 3.8 %fusion = bf16[1024,1024]{1,0:T(8,128)(2,1)} fusion(bf16[1024,1024]{1,0:T(8,128)(2,1)} %bitcast.16, f32[]{:T(128)} %bitcast.2, bf16[4096,256]{1,0:T(8,128)(2,1)S(1)} %copy-done, s32[]{:T(128)S(6)} %select_n.15, bf16[256,3072]{1,0:T(8,128)(2,1)} %bitcast.11), kind=kOutput, calls=%fused_computation.1 | convolution fusion | flops 541065216 | bytes 5243396 | tf_op jit(solution)/shard_map/dot_general | solution.py:323
  90.7 4.0 %fusion.1 = bf16[512,2048]{1,0:T(8,128)(2,1)} fusion(bf16[512,2048]{1,0:T(8,128)(2,1)} %bitcast.15, f32[]{:T(128)} %bitcast, bf16[256,3072]{1,0:T(8,128)(2,1)} %bitcast.12, bf16[2048,256]{1,0:T(8,128)(2,1)S(1)} %copy-done.8, s32[]{:T(128)S(6)} %select_n.14), kind=kOutput, calls=%fused_computation.3 | convolution fusion | flops 541065216 | bytes 5505540 | tf_op jit(solution)/shard_map/dot_general | solution.py:323
  94.6 2.3 %convolution_multiply_fusion.1 = f32[256,1024]{1,0:T(8,128)} fusion(f32[]{:T(128)} %bitcast.2, bf16[256,3072]{1,0:T(8,128)(2,1)} %bitcast.13, bf16[4096,256]{1,0:T(8,128)(2,1)S(1)} %copy-done, s32[]{:T(128)S(6)} %select_n.13), kind=kOutput, calls=%fused_computation.5 | convolution fusion | flops 134479872 | bytes 1704452 | tf_op jit(solution)/shard_map/dot_general | solution.py:322
  97.0 2.5 %convolution_multiply_fusion = f32[128,2048]{1,0:T(8,128)} fusion(bf16[256,3072]{1,0:T(8,128)(2,1)} %bitcast.14, f32[]{:T(128)} %bitcast, bf16[2048,256]{1,0:T(8,128)(2,1)S(1)} %copy-done.8, s32[]{:T(128)S(6)} %select_n.12), kind=kOutput, calls=%fused_computation.4 | convolution fusion | flops 134479872 | bytes 2163204 | tf_op jit(solution)/shard_map/dot_general | solution.py:322
  99.5 0.7 copy.24
  100.1 0.7 copy.25
  100.8 0.6 copy.26
  101.4 0.6 copy.27
Async XLA Ops:
  0.6 1.6 %copy-start = (bf16[4096,256]{1,0:T(8,128)(2,1)S(1)}, bf16[4096,256]{1,0:T(8,128)(2,1)}, u32[]{:S(2)}) copy-start(bf16[4096,256]{1,0:T(8,128)(2,1)} %param.17) | copy-start | bytes 6291460
  0.6 7.9 %copy-start.9 = (bf16[1024,2048]{1,0:T(8,128)(2,1)S(1)}, bf16[1024,2048]{1,0:T(8,128)(2,1)}, u32[]{:S(2)}) copy-start(bf16[1024,2048]{1,0:T(8,128)(2,1)} %param.12) | copy-start | bytes 12582916
  0.7 7.9 %copy-start.8 = (bf16[2048,256]{1,0:T(8,128)(2,1)S(1)}, bf16[2048,256]{1,0:T(8,128)(2,1)}, u32[]{:S(2)}) copy-start(bf16[2048,256]{1,0:T(8,128)(2,1)} %param.16) | copy-start | bytes 3145732
  9.9 1.2 %copy-start.6 = (f32[128,2048]{1,0:T(8,128)S(1)}, f32[128,2048]{1,0:T(8,128)}, u32[]{:S(2)}) copy-start(f32[128,2048]{1,0:T(8,128)} %param.18) | copy-start | bytes 3145732
  9.9 1.5 %copy-start.7 = (f32[256,1024]{1,0:T(8,128)S(1)}, f32[256,1024]{1,0:T(8,128)}, u32[]{:S(2)}) copy-start(f32[256,1024]{1,0:T(8,128)} %param.19) | copy-start | bytes 3145732
  10.1 1.4 %copy-start.2 = (f32[16,2048]{1,0:T(8,128)S(1)}, f32[16,2048]{1,0:T(8,128)}, u32[]{:S(2)}) copy-start(f32[16,2048]{1,0:T(8,128)} %first_in.1) | copy-start | bytes 393220
  10.1 1.4 %copy-start.3 = (f32[16,2048]{1,0:T(8,128)S(1)}, f32[16,2048]{1,0:T(8,128)}, u32[]{:S(2)}) copy-start(f32[16,2048]{1,0:T(8,128)} %second_in.1) | copy-start | bytes 393220
  10.1 1.4 %copy-start.4 = (f32[16,1024]{1,0:T(8,128)S(1)}, f32[16,1024]{1,0:T(8,128)}, u32[]{:S(2)}) copy-start(f32[16,1024]{1,0:T(8,128)} %first_mid.1) | copy-start | bytes 196612
  10.1 1.4 %copy-start.5 = (f32[16,1024]{1,0:T(8,128)S(1)}, f32[16,1024]{1,0:T(8,128)}, u32[]{:S(2)}) copy-start(f32[16,1024]{1,0:T(8,128)} %second_mid.1) | copy-start | bytes 196612
  83.8 1.2 %copy-start.1 = (bf16[4,4,16,3072]{3,2,1,0:T(8,128)(2,1)}, bf16[4,4,16,3072]{3,2,1,0:T(8,128)(2,1)S(1)}, u32[]{:S(2)}) copy-start(bf16[4,4,16,3072]{3,2,1,0:T(8,128)(2,1)S(1)} %get-tuple-element.17) | copy-start | bytes 4718596

commit v2 on v1

--- a/solution.py
+++ b/solution.py
@@ -22,11 +22,12 @@
 
 def exchange(
     sizes,
-    low_in, low_mid, cot_in, cot_mid, master_in, master_mid,
+    normed, gated, basis_in, basis_mid, cot_in, cot_mid, exact_in, exact_mid,
     first_in, second_in, first_mid, second_mid,
     ways, weights_in, weights_mid, moment_in, square_in, moment_mid, square_mid, totals,
+    full_in, full_mid, master_in, master_mid, tall_in, tall_mid, left_in, left_mid, low_in, low_mid,
     cots, whole, own, part, zland, spread, xland, sums,
-    cot_sem, zsend, zrecv, xsend, xrecv, msend, mrecv, mlocal, gzs, gxs, gys, gdiag, grecv, tsend, trecv,
+    load_sem, left_sem, cot_sem, zsend, zrecv, xsend, xrecv, msend, mrecv, mlocal, gzs, gxs, gys, gdiag, grecv, tsend, trecv,
 ):
     F, R, T, rows, width, n_in, n_mid = sizes
     nt = n_in + n_mid
@@ -39,12 +40,33 @@
             source.at[:, pl.ds(pl.multiple_of((c - base) * width, width), width)], cots.at[c], cot_sem.at[c]
         )
 
-    for c in range(nt):
-        (cot_copy(c, cot_in, 0) if c < n_in else cot_copy(c, cot_mid, n_in)).start()
+    steps = left_sem.shape[1]
+    deep = normed.shape[0] // steps
+
+    def left_copy(which, k):
+        source, target = ((normed, left_in), (gated, left_mid))[which]
+        span = pl.ds(pl.multiple_of(k * deep, deep), deep)
+        return pltpu.make_async_copy(source.at[span], target.at[span], left_sem.at[which, k])
+
+    loads = [
+        pltpu.make_async_copy(exact_in, full_in, load_sem.at[0]),
+        pltpu.make_async_copy(exact_mid, full_mid, load_sem.at[1]),
+        pltpu.make_async_copy(basis_in, tall_in, load_sem.at[2]),
+        pltpu.make_async_copy(basis_mid, tall_mid, load_sem.at[3]),
+    ]
+    for load in loads[:3]:
+        load.start()
+    for k in range(steps):
+        left_copy(0, k).start()
+    for c in range(n_in):
+        cot_copy(c, cot_in, 0).start()
+    loads[3].start()
+    for k in range(steps):
+        left_copy(1, k).start()
+    for c in range(n_in, nt):
+        cot_copy(c, cot_mid, n_in).start()
     local_in = pltpu.make_async_copy(master_in, weights_in.at[r], mlocal.at[0])
     local_mid = pltpu.make_async_copy(master_mid, weights_mid.at[r], mlocal.at[1])
-    local_in.start()
-    local_mid.start()
 
     barrier = pltpu.get_barrier_semaphore()
     for k in range(1, F):
@@ -53,6 +75,10 @@
         pl.semaphore_signal(barrier, inc=1, device_id={"rep": lax.rem(r + k, R)}, device_id_type=MESH)
     for k in range(1, T):
         pl.semaphore_signal(barrier, inc=1, device_id={"tp": lax.rem(t + k, T)}, device_id_type=MESH)
+    loads[0].wait()
+    master_in[...] = full_in[...].astype(jnp.bfloat16)
+    loads[1].wait()
+    master_mid[...] = full_mid[...].astype(jnp.bfloat16)
     pl.semaphore_wait(barrier, F + R + T - 3)
 
     half = R // 2
@@ -81,6 +107,21 @@
     ]
     for copy in m_sends:
         copy.start()
+    local_in.start()
+    local_mid.start()
+
+    def lower(which, tall, low_ref):
+        loads[2 + which].wait()
+
+        @pl.loop(0, steps)
+        def _(k):
+            left_copy(which, k).wait()
+            span = pl.ds(pl.multiple_of(k * deep, deep), deep)
+            left = (left_in, left_mid)[which]
+            low = jnp.dot(left[span, :], tall[...], preferred_element_type=jnp.float32).T
+            upper = low.astype(jnp.bfloat16)
+            low_ref[:rank, span] = upper
+            low_ref[rank:, span] = (low - upper.astype(jnp.float32)).astype(jnp.bfloat16)
 
     def z_copy(c, peer, slot, to):
         return remote(part.at[c, peer], zland.at[c, slot], zsend.at[c, peer], zrecv.at[c, slot], {"fs": to})
@@ -96,9 +137,13 @@
             peer = lax.rem(f + k, F)
             z_copy(c, peer, f, peer).start()
 
+    lower(0, tall_in, low_in)
+
     @pl.loop(0, n_in)
     def _(c):
         contract(low_in, cot_in, 0, c)
+
+    lower(1, tall_mid, low_mid)
 
     @pl.loop(n_in, nt)
     def _(c):
@@ -248,17 +293,6 @@
     n_in, n_mid = cols_in // width, cols_mid // width
     nt = n_in + n_mid
 
-    def split(basis, inputs):
-        lowered = lax.dot_general(basis, inputs, (((0,), (1,)), ((), ())), preferred_element_type=jnp.float32)
-        upper = lowered.astype(jnp.bfloat16)
-        lower = (lowered - upper.astype(jnp.float32)).astype(jnp.bfloat16)
-        return jnp.concatenate([upper, lower], axis=0)
-
-    low_in = split(basis_in, normed_in)
-    low_mid = split(basis_mid, gated_mid)
-    rough_in = master_in.astype(jnp.bfloat16)
-    rough_mid = master_mid.astype(jnp.bfloat16)
-
     vmem = pl.BlockSpec(memory_space=pltpu.VMEM)
     anywhere = pl.BlockSpec(memory_space=pl.ANY)
     dma = pltpu.SemaphoreType.DMA
@@ -276,9 +310,19 @@
             small(first_mid.shape, f32),
             small((2, 8, 128), f32),
         ),
-        in_specs=[vmem, vmem, anywhere, anywhere, vmem, vmem, vmem, vmem, vmem, vmem],
+        in_specs=[anywhere] * 8 + [vmem] * 4,
         out_specs=(vmem, anywhere, anywhere, vmem, vmem, vmem, vmem, vmem),
         scratch_shapes=[
+            pltpu.VMEM(master_in.shape, f32),
+            pltpu.VMEM(master_mid.shape, f32),
+            pltpu.VMEM(master_in.shape, bf16),
+            pltpu.VMEM(master_mid.shape, bf16),
+            pltpu.VMEM(basis_in.shape, bf16),
+            pltpu.VMEM(basis_mid.shape, bf16),
+            pltpu.VMEM(normed_in.shape, bf16),
+            pltpu.VMEM(gated_mid.shape, bf16),
+            pltpu.VMEM((2 * rank, tokens), bf16),
+            pltpu.VMEM((2 * rank, tokens), bf16),
             pltpu.VMEM((nt, tokens, width), bf16),
             pltpu.VMEM((F, R * rows, width), f32),
             pltpu.VMEM((nt, R * rows, width), f32),
@@ -287,6 +331,8 @@
             pltpu.VMEM((nt, R, rows, width), f32),
             pltpu.VMEM((nt, R, rows, width), f32),
             pltpu.VMEM((T, 2, 8, 128), f32),
+            dma((4,)),
+            dma((2, tokens // 512)),
             dma((nt,)),
             dma((nt, F)),
             dma((nt, F)),
@@ -304,29 +350,102 @@
             dma((T,)),
         ],
         compiler_params=pltpu.CompilerParams(
-            collective_id=0, has_side_effects=True, vmem_limit_bytes=48 * 1024 * 1024
+            collective_id=0, has_side_effects=True, vmem_limit_bytes=56 * 1024 * 1024
         ),
     )(
-        low_in, low_mid, inner_cot, output_cot, rough_in, rough_mid,
+        normed_in, gated_mid, basis_in, basis_mid, inner_cot, output_cot, master_in, master_mid,
         first_in, second_in, first_mid, second_mid,
     )
 
-    f, slot = lax.axis_index("fs"), lax.axis_index(("fs", "rep"))
-    flat = ways.reshape(rank, nt * width)
-
-    def finish(total, columns, basis, master, weights, way):
-        scale = rate_scale * lax.rsqrt(total / (rank * columns * T) + 1e-06)
-        count = master.shape[0]
-        mine = lax.dynamic_slice_in_dim(basis, slot * count, count, 0)
-        group = lax.dynamic_slice_in_dim(basis, f * count * R, count * R, 0)
-        step = scale * jnp.dot(mine, way, preferred_element_type=f32)
-        course = scale * jnp.dot(group, way, preferred_element_type=f32)
-        copy = (weights.reshape(count * R, columns).astype(f32) - course).astype(bf16)
-        return step, copy
-
-    step_in, copy_in = finish(totals[0, 0, 0], cols_in, basis_in, master_in, weights_in, flat[:, :cols_in])
-    step_mid, copy_mid = finish(totals[1, 0, 0], cols_mid, basis_mid, master_mid, weights_mid, flat[:, cols_in:])
-    return (step_in, step_mid, moment_in, square_in, moment_mid, square_mid, copy_in, copy_mid)
+    where = jnp.stack([lax.axis_index("fs"), lax.axis_index("rep")]).astype(jnp.int32)
+    tall_in, tall_mid = master_in.shape[0], master_mid.shape[0]
+
+    def block(shape, turn):
+        return pl.BlockSpec(shape, turn)
+
+    def turned(j, at):
+        return lax.rem(at[1] + j, R)
+
+    def still(shape):
+        return pl.BlockSpec(shape, lambda j, at: (0,) * len(shape))
+
+    small_specs = [still(x.shape) for x in (moment_in, square_in, moment_mid, square_mid)]
+    results = pl.pallas_call(
+        functools.partial(finish, (rank * cols_in * T, rank * cols_mid * T, cols_in)),
+        grid_spec=pltpu.PrefetchScalarGridSpec(
+            num_scalar_prefetch=1,
+            grid=(R,),
+            in_specs=[
+                still((2, 8, 128)),
+                still((rank, nt * width)),
+                block((tall_in, rank), lambda j, at: (at[0] * R + turned(j, at), 0)),
+                block((tall_mid, rank), lambda j, at: (at[0] * R + turned(j, at), 0)),
+                block((1, tall_in, cols_in), lambda j, at: (turned(j, at), 0, 0)),
+                block((1, tall_mid, cols_mid), lambda j, at: (turned(j, at), 0, 0)),
+                *small_specs,
+            ],
+            out_specs=[
+                anywhere,
+                anywhere,
+                *small_specs,
+                block((tall_in, cols_in), lambda j, at: (turned(j, at), 0)),
+                block((tall_mid, cols_mid), lambda j, at: (turned(j, at), 0)),
+            ],
+            scratch_shapes=[
+                pltpu.VMEM(master_in.shape, f32),
+                pltpu.VMEM(master_mid.shape, f32),
+                dma((2,)),
+            ],
+        ),
+        out_shape=[
+            small(master_in.shape, f32),
+            small(master_mid.shape, f32),
+            small(first_in.shape, f32),
+            small(first_in.shape, f32),
+            small(first_mid.shape, f32),
+            small(first_mid.shape, f32),
+            small((R * tall_in, cols_in), bf16),
+            small((R * tall_mid, cols_mid), bf16),
+        ],
+        compiler_params=pltpu.CompilerParams(vmem_limit_bytes=56 * 1024 * 1024),
+    )(
+        where, totals, ways.reshape(rank, nt * width), basis_in, basis_mid, weights_in, weights_mid,
+        moment_in, square_in, moment_mid, square_mid,
+    )
+    return tuple(results)
+
+
+def finish(
+    counts, at, totals, way, basis_in, basis_mid, weights_in, weights_mid, *rest
+):
+    small_in, (step_in, step_mid), small_out = rest[:4], rest[4:6], rest[6:10]
+    copy_in, copy_mid, held_in, held_mid, sems = rest[10:]
+    turn = pl.program_id(0)
+    out_in = pltpu.make_async_copy(held_in, step_in, sems.at[0])
+    out_mid = pltpu.make_async_copy(held_mid, step_mid, sems.at[1])
+    sides = (
+        (0, counts[0], basis_in, weights_in, copy_in, held_in, out_in, slice(0, counts[2])),
+        (1, counts[1], basis_mid, weights_mid, copy_mid, held_mid, out_mid, slice(counts[2], None)),
+    )
+    for side, count, basis, weights, copy, held, out, span in sides:
+        scale = rate_scale * lax.rsqrt(totals[side, 0:1, 0:1] / count + 1e-06)
+        step = scale * jnp.dot(basis[...], way[:, span], preferred_element_type=jnp.float32)
+        copy[...] = (weights[0].astype(jnp.float32) - step).astype(jnp.bfloat16)
+
+        @pl.when(turn == 0)
+        def _():
+            held[...] = step
+            out.start()
+
+    @pl.when(turn == 0)
+    def _():
+        for source, target in zip(small_in, small_out):
+            target[...] = source[...]
+
+    @pl.when(turn == pl.num_programs(0) - 1)
+    def _():
+        out_in.wait()
+        out_mid.wait()
 
 
 def solution(mesh):

time: 102 us -> 89.5 us (0.88)
  matrix products: 20.2 us -> 0 us
  Pallas kernels: 72.2 us -> 88.1 us
  local copies, waits for them, and re-layouts: 7.11 us -> 0 us
  between operations: 2.21 us -> 0.65 us
    dot_general x6 -> x0, matrix products: 20.2 us -> none  [the longest x2 7.77 us: finish(): course = scale * jnp.dot(group, way, preferred_element_type=f32)]
    pallas_call x0 -> x1, Pallas kernels: none -> 8.26 us  [body(): pl.pallas_call(functools.partial(finish, (rank * cols_in * T, rank * cols...]
    pallas_call x1, Pallas kernels: 72.2 us -> 79.9 us  [body(): pl.pallas_call(functools.partial(exchange, (F, R, T, rows, width, n_in, n...]
    unnamed x24 -> x0, local copies, waits for them, and re-layouts: 6.59 us -> none
where the time goes in v2:
time: 89.5 us; the launch traced here: 89.3 us
  Pallas kernels  88.1 us (98%)
    pallas_call x1, Pallas kernels, body(): pl.pallas_call(functools.partial(exchange, (F, R, T, rows, width, n_in, n...  79.9 us
    pallas_call x1, Pallas kernels, body(): pl.pallas_call(functools.partial(finish, (rank * cols_in * T, rank * cols...  8.26 us

profile of v2, /device:TPU:0, one launch (start us, length us, event | category | flops | bytes accessed | tf_op | source)
XLA Modules:
  0.0 89.3 jit_solution(7158791687356018763)
XLA Ops:
  0.6 0.6 pad_add_fusion.at
  1.2 79.9 %shard_map.179 = (bf16[4,4,16,3072]{3,2,1,0:T(8,128)(2,1)}, bf16[4,128,2048]{2,1,0:T(8,128)(2,1)}, bf16[4,256,1024]{2,1,0:T(8,128)(2,1)}, f32[16,2048]{1,0:T(8,1...) custom-call(bf16[1024,2048]{1,0:T(8,128)(2,1)} %normed.1, ...), custom_call_target="tpu_custom_call" | custom-call | tf_op jit(solution)/shard_map/pallas_call | solution.py:301
  81.1 8.3 %shard_map.180 = (f32[128,2048]{1,0:T(8,128)}, f32[256,1024]{1,0:T(8,128)}, f32[16,2048]{1,0:T(8,128)}, f32[16,2048]{1,0:T(8,128)}, f32[16,1024]{1,0:T(8,128)}, ...) custom-call(s32[2]{0:T(128)} %pad_add_fusion.at, ...), custom_call_target="tpu_custom_call" | custom-call | tf_op jit(solution)/shard_map/pallas_call | solution.py:373
